TPU v7x, 256 devices: a whole 4x4x8 slice. The times are simulated.
256 devices in a mesh: ep: 64 (over z, x, core), tp: 4 (over y).
Axes of the slice: x: 4, y: 4, z: 8, core: 2. Of those that a mesh axis runs over, the one named last changes fastest.
Arguments:
- mixer_input: bfloat16 [32768, 2048], P('ep'), may hold values from -5.5 to 5.5
- expert_input: bfloat16 [32768, 2048], P('ep'), may hold values from -6 to 6
- gain_mixer: float32 [2048], replicated, may hold values from 0.1 to 1.9
- gain_expert: float32 [2048], replicated, may hold values from 0.1 to 1.9
- query_weight: bfloat16 [2048, 1536], P(None, 'tp')
- key_weight: bfloat16 [2048, 256], P(None, 'tp')
- value_weight: bfloat16 [2048, 256], P(None, 'tp'), may hold values from -0.125 to 0.125
- sink_logits: float32 [24], P('tp'), may hold values from 2 to 6
- output_weight: bfloat16 [1536, 2048], P('tp'), may hold values from -0.75 to 0.75
- expert_choice: int32 [32768, 2], P('ep'), may hold values from 0 to 63, all different within a row; in each aligned block of 128 rows (0 to 127, 128 to 255, ...) at most 8 rows name the same one
- route_weights: float32 [32768, 2], P('ep'), may hold values from 0.2 to 1.2
- expert_gate: bfloat16 [64, 2048, 1024], P('ep', None, 'tp'), may hold values from -0.125 to 0.125
- expert_up: bfloat16 [64, 2048, 1024], P('ep', None, 'tp'), may hold values from -0.125 to 0.125
- expert_down: bfloat16 [64, 1024, 2048], P('ep', 'tp'), may hold values from -0.1875 to 0.1875
- shared_gate: bfloat16 [2048, 512], P(None, 'tp'), may hold values from -0.125 to 0.125
- shared_up: bfloat16 [2048, 512], P(None, 'tp'), may hold values from -0.125 to 0.125
- shared_down: bfloat16 [512, 2048], P('tp'), may hold values from -0.25 to 0.25
Outputs:
- mixer_output: bfloat16 [32768, 2048], P(('ep', 'tp'))
- expert_output: bfloat16 [32768, 2048], P(('ep', 'tp'))
Inputs may be any that keep to these rules, and one draw needn't show every extreme that they name: `expert_choice`: in each aligned block of 128 rows no expert is named by more than 8 rows, and in some block some expert is named by exactly 8 rows; the 2 entries of a row differ.
All inputs are finite; a program needn't handle non-finite values.
Results may differ from a plain program's by a relative error of at most 0.019.
Values may be sent and summed in bfloat16 or wider, within the bound.
A program may use at most 128 MiB of HBM per device.

v0:
```python
import math
import jax
import jax.numpy as jnp
from jax import lax
from jax.sharding import PartitionSpec as P

HEAD_DIM = 64
WINDOW = 128
SEQS = 1
norm_eps = 1e-06
rope_base = 500000.0


def from_behind(value, axis, steps):
    count = lax.axis_size(axis)
    first, last = (max(0, -steps), min(count, count - steps))
    return lax.ppermute(value, axis, [(source, source + steps) for source in range(first, last)])


def cut_along(shard, dim, count):
    lengths = shard.shape
    pieces = shard.reshape(*lengths[:dim], count, lengths[dim] // count, *lengths[dim + 1 :])
    return jnp.moveaxis(pieces, dim, 0)


def sent_and_summed(shard, axis, dim):
    pieces = cut_along(shard, dim, lax.axis_size(axis))
    arrived = lax.all_to_all(pieces, axis, split_axis=0, concat_axis=0, tiled=True)
    return arrived.astype(jnp.float32).sum(axis=0)


def rounded(value):
    return lax.optimization_barrier(value.astype(jnp.bfloat16)).astype(jnp.float32)


def rms_scale(matrix, scaling):
    widened = matrix.astype(jnp.float32)
    scaled = widened * lax.rsqrt(jnp.mean(widened * widened, axis=-1, keepdims=True) + norm_eps)
    return (scaled * scaling).astype(jnp.bfloat16)


def frequencies(head_size):
    half_steps = jnp.arange(head_size // 2, dtype=jnp.float32)
    return rope_base ** (-(2.0 * half_steps) / head_size)


def rotate(heads, angles):
    middle = heads.shape[-1] // 2
    widened = heads.astype(jnp.float32)
    cosine = jnp.cos(angles)[:, None, :]
    sine_val = jnp.sin(angles)[:, None, :]
    leading = widened[..., :middle]
    trailing = widened[..., middle:]
    turned = jnp.concatenate(
        [leading * cosine - trailing * sine_val, trailing * cosine + leading * sine_val], axis=-1
    )
    return turned.astype(jnp.bfloat16)


def attend(
    query_heads, key_heads, value_heads, prior_keys, prior_values, first_position, sink_logits
):
    window = prior_keys.shape[0]
    total_rows, kv_count, head_size = key_heads.shape
    group_size = query_heads.shape[1] // kv_count
    blocks = total_rows // window

    def banded(earlier, current):
        joined = jnp.concatenate([earlier, current], axis=0).reshape(
            blocks + 1, window, kv_count, head_size
        )
        return jnp.concatenate([joined[:-1], joined[1:]], axis=1)

    band_keys = banded(prior_keys, key_heads)
    band_values = banded(prior_values, value_heads)
    query_blocks = query_heads.reshape(blocks, window, kv_count, group_size, head_size)
    scores = jnp.einsum(
        "nqhgd,nkhd->nhgqk", query_blocks, band_keys, preferred_element_type=jnp.float32
    ) / math.sqrt(head_size)
    query_index = jnp.arange(window, dtype=jnp.int32)[:, None]
    key_index = jnp.arange(2 * window, dtype=jnp.int32)[None, :]
    distance = query_index + window - key_index
    block_start = first_position + jnp.arange(blocks, dtype=jnp.int32)[:, None, None] * window
    allowed = (distance >= 0) & (distance < window) & (block_start - window + key_index >= 0)
    scores = jnp.where(allowed[:, None, None, :, :], scores, -jnp.inf)
    sink_grid = sink_logits.reshape(kv_count, group_size)[None, :, :, None, None]
    row_peak = jnp.maximum(jnp.max(scores, axis=-1, keepdims=True), sink_grid)
    shifted_exp = jnp.exp(scores - row_peak)
    denominator = jnp.sum(shifted_exp, axis=-1, keepdims=True) + jnp.exp(sink_grid - row_peak)
    probs = (shifted_exp / denominator).astype(jnp.bfloat16)
    attended = jnp.einsum(
        "nhgqk,nkhd->nqhgd", probs, band_values, preferred_element_type=jnp.float32
    )
    return attended.astype(jnp.bfloat16).reshape(total_rows, kv_count * group_size * head_size)


def local(
    mixer_input,
    expert_input,
    gain_mixer,
    gain_expert,
    query_weight,
    key_weight,
    value_weight,
    sink_logits,
    output_weight,
    expert_choice,
    route_weights,
    expert_gate,
    expert_up,
    expert_down,
    shared_gate,
    shared_up,
    shared_down,
):
    tp_count = lax.axis_size("tp")
    ep_count = lax.axis_size("ep")
    tp_rank = lax.axis_index("tp")
    group_rows, model_width = mixer_input.shape
    normed = rms_scale(mixer_input, gain_mixer)
    queries = jnp.dot(normed, query_weight, preferred_element_type=jnp.float32).astype(jnp.bfloat16)
    key_rows = jnp.dot(normed, key_weight, preferred_element_type=jnp.float32).astype(jnp.bfloat16)
    value_rows = jnp.dot(normed, value_weight, preferred_element_type=jnp.float32).astype(
        jnp.bfloat16
    )
    first_position = lax.axis_index("ep") % (ep_count // SEQS) * group_rows
    positions = (first_position + jnp.arange(group_rows, dtype=jnp.int32)).astype(jnp.float32)
    angles = positions[:, None] * frequencies(HEAD_DIM)[None, :]
    rot_queries = rotate(queries.reshape(group_rows, -1, HEAD_DIM), angles)
    rot_keys = rotate(key_rows.reshape(group_rows, -1, HEAD_DIM), angles)
    key_width = key_rows.shape[1]
    tail_start = group_rows - WINDOW
    tail_pair = jnp.concatenate(
        [rot_keys.reshape(group_rows, key_width)[tail_start:], value_rows[tail_start:]], axis=1
    )
    earlier_pair = from_behind(tail_pair, "ep", 1)
    prior_keys = earlier_pair[:, :key_width].reshape(WINDOW, -1, HEAD_DIM)
    prior_values = earlier_pair[:, key_width:].reshape(WINDOW, -1, HEAD_DIM)
    attended = attend(
        rot_queries,
        rot_keys,
        value_rows.reshape(group_rows, -1, HEAD_DIM),
        prior_keys,
        prior_values,
        first_position,
        sink_logits,
    )
    picked = attended
    mixer_output = lax.psum_scatter(
        rounded(jnp.dot(picked, output_weight, preferred_element_type=jnp.float32)).astype(
            jnp.bfloat16
        ),
        "tp",
        scatter_dimension=0,
        tiled=True,
    )
    normed_rows = rms_scale(expert_input, gain_expert)
    group_tokens = normed_rows.shape[0]
    own_tokens = group_tokens // tp_count
    top_count = expert_choice.shape[1]
    local_experts = expert_gate.shape[0]
    experts_all = local_experts * ep_count
    capacity = 2 * own_tokens * top_count // experts_all
    assigned = own_tokens * top_count
    picked_experts = expert_choice.reshape(tp_count, assigned)
    onehot = (
        picked_experts[:, :, None] == jnp.arange(experts_all, dtype=jnp.int32)[None, None, :]
    ).astype(jnp.int32)
    slot_ranks = jnp.sum(jnp.cumsum(onehot, axis=1) * onehot, axis=-1) - 1
    padded_rows = jnp.concatenate([normed_rows, jnp.zeros((1, model_width), jnp.bfloat16)], axis=0)

    def own_slot_index():
        own_experts = lax.dynamic_index_in_dim(picked_experts, tp_rank, 0, keepdims=False)
        own_ranks = lax.dynamic_index_in_dim(slot_ranks, tp_rank, 0, keepdims=False)
        return own_experts * capacity + own_ranks

    own_owner = tp_rank * own_tokens + jnp.arange(assigned, dtype=jnp.int32) // top_count
    slot_table = (
        jnp.full((experts_all * capacity,), group_tokens, jnp.int32)
        .at[own_slot_index()]
        .set(own_owner)
    )
    outgoing = padded_rows[slot_table].reshape(experts_all, 1, capacity, model_width)
    arrived = lax.all_gather(
        lax.all_to_all(outgoing, "ep", split_axis=0, concat_axis=0, tiled=True),
        "tp",
        axis=1,
        tiled=True,
    )
    sources = arrived.shape[0] // local_experts
    shaped = arrived.reshape(
        sources, local_experts, arrived.shape[1], arrived.shape[2], arrived.shape[3]
    )
    gate_values = jnp.einsum(
        "iejcd,edf->iejcf", shaped, expert_gate, preferred_element_type=jnp.float32
    )
    up_values = jnp.einsum(
        "iejcd,edf->iejcf", shaped, expert_up, preferred_element_type=jnp.float32
    )
    hidden = (jax.nn.silu(gate_values) * up_values).astype(jnp.bfloat16)
    result = jnp.einsum("iejcf,efd->iejcd", hidden, expert_down, preferred_element_type=jnp.float32)
    partials = result.astype(jnp.bfloat16).reshape(arrived.shape)
    summed = sent_and_summed(partials.astype(jnp.float32).astype(jnp.bfloat16), "tp", 1)
    returned = (
        lax.all_to_all(summed.astype(jnp.bfloat16), "ep", split_axis=0, concat_axis=0, tiled=True)
        .astype(summed.dtype)
        .reshape(-1, model_width)
    )
    own_weights = lax.dynamic_slice_in_dim(route_weights, tp_rank * own_tokens, own_tokens, 0)
    gathered = returned[own_slot_index().reshape(own_tokens, top_count)]
    routed = jnp.sum(gathered * own_weights[:, :, None], axis=1)
    picked = normed_rows
    gate_values = jnp.dot(picked, shared_gate, preferred_element_type=jnp.float32)
    up_values = jnp.dot(picked, shared_up, preferred_element_type=jnp.float32)
    hidden = (jax.nn.silu(gate_values) * up_values).astype(jnp.bfloat16)
    shared_part = lax.psum_scatter(
        rounded(jnp.dot(hidden, shared_down, preferred_element_type=jnp.float32)).astype(
            jnp.bfloat16
        ),
        "tp",
        scatter_dimension=0,
        tiled=True,
    ).astype(jnp.float32)
    expert_output = (routed + shared_part).astype(jnp.bfloat16)
    return (mixer_output, expert_output)


def solution(mesh):
    placed = (
        P("ep", None),
        P("ep", None),
        P(),
        P(),
        P(None, "tp"),
        P(None, "tp"),
        P(None, "tp"),
        P("tp"),
        P("tp", None),
        P("ep", None),
        P("ep", None),
        P("ep", None, "tp"),
        P("ep", None, "tp"),
        P("ep", "tp", None),
        P(None, "tp"),
        P(None, "tp"),
        P("tp", None),
    )
    return jax.shard_map(
        local,
        mesh=mesh,
        in_specs=placed,
        out_specs=(P(("ep", "tp"), None), P(("ep", "tp"), None)),
        check_vma=False,
    )
```

profile of v0, /device:TPU:2, one launch (start us, length us, event | category | flops | bytes accessed | tf_op | source)
XLA Modules:
  0.0 415.3 jit_solution(7231487003897511812)
XLA Ops:
  10.7 2.4 reduce-window.6
  16.1 2.1 fusion.5
  21.2 7.1 %gather_fusion = bf16[512,2048]{1,0:T(8,128)(2,1)} fusion(bf16[513,2048]{1,0:T(8,128)(2,1)} %concatenate.64, s32[1024]{0:T(1024)S(1)} %pad_clamp_fusion.1), kind=kCustom, calls=%fused_computation | custom fusion | bytes 4196352 | tf_op jit(solution)/shard_map/gather | solution.py:183
  28.3 63.5 %all_to_all.15 = bf16[64,1,8,2048]{3,2,1,0:T(8,128)(2,1)} all-to-all(bf16[64,1,8,2048]{3,2,1,0:T(8,128)(2,1)} %bitcast.203), channel_id=1, replica_groups=mesh['ep'=64,'tp'=4] {'ep'}, dimensions={0} | all-to-all | bytes 4194304 | tf_op jit(solution)/shard_map/all_to_all | solution.py:185
  91.8 82.2 %all-gather.2.cloned.1.call-done = bf16[64,4,8,2048]{3,2,1,0:T(8,128)(2,1)} async-done(((bf16[64,1,8,2048]{3,2,1,0:T(8,128)(2,1)}), bf16[64,4,8,2048]{3,2,1,0:T(8,128)(2,1)}) %all-gather.2.cloned.1.call-update) | async-done | bytes 8388624 | tf_op jit(solution)/shard_map/all_gather | solution.py:184
  174.0 7.1 %fusion.27 = f32[64,4,8,256]{3,2,1,0:T(8,128)} fusion(bf16[64,4,8,2048]{3,2,1,0:T(8,128)(2,1)} %all-gather.2.cloned.1.call-done, bf16[1,2048,256]{2,1,0:T(8,128)(2,1)S(1)} %copy-done.10), kind=kOutput, calls=%fused_computation.45 | convolution fusion | flops 2147483648 | bytes 11534336 | tf_op jit(solution)/shard_map/iejcd,edf->iejcf/dot_general | solution.py:194
  181.1 13.7 %convert_bitcast_fusion = bf16[4,64,1,8,2048]{4,3,0,1,2:T(8,128)(2,1)} fusion(bf16[1,256,2048]{2,1,0:T(8,128)(2,1)} %param.30, bf16[64,4,8,2048]{3,2,1,0:T(8,128)(2,1)} %all-gather.2.cloned.1.call-done, f32[64,4,8,256]{3,2,1,0:T(8,128)} %fusion.27, bf16[1,2048,256]{2,1,0:T(8,128)(2,1)} %param.29), kind=kOutput, calls=%fused_computation.3 | convolution fusion | flops 4302307328 | bytes 20971520 | tf_op jit(solution)/shard_map/iejcf,efd->iejcd/dot_general | solution.py:201
  194.8 8.3 %copy.55 = bf16[4,64,1,8,2048]{4,3,1,2,0:T(8,128)(2,1)} copy(bf16[4,64,1,8,2048]{4,3,0,1,2:T(8,128)(2,1)} %convert_bitcast_fusion) | data formatting | bytes 16777216 | tf_op jit(solution)/shard_map/transpose | solution.py:23
  203.1 5.7 %all-to-all-start.1 = ((bf16[4,64,1,8,2048]{4,3,1,2,0:T(8,128)(2,1)}), bf16[4,64,1,8,2048]{4,3,1,2,0:T(8,128)(2,1)}, u32[]{:S(2)}, u32[]{:S(2)}) async-start(bf16[4,64,1,8,2048]{4,3,1,2,0:T(8,128)(2,1)} %copy.55), calls=%async_computation.2 | async-start | bytes 16777216 | tf_op jit(solution)/shard_map/all_to_all | solution.py:28
  211.0 2.6 convolution_convert_fusion.3
  214.8 2.1 collective-permute-start
  217.7 5.3 %convolution_convert_fusion = bf16[512,2048]{1,0:T(8,128)(2,1)} fusion(bf16[128,2048]{1,0:T(8,128)(2,1)S(1)} %copy-done.6, bf16[512,2048]{1,0:T(8,128)(2,1)} %copy-done.1, bf16[2048,128]{1,0:T(8,128)(2,1)S(1)} %copy-done.7, f32[512,128]{1,0:T(8,128)S(1)} %fusion.85), kind=kOutput, calls=%fused_computation.17 | convolution fusion | flops 538312704 | bytes 5505024 | tf_op jit(solution)/shard_map/dot_general | solution.py:217
  223.0 3.2 convolution_convert_fusion.2
  227.3 2.3 fusion.7
  229.7 89.8 %all-to-all-done.1 = bf16[4,64,1,8,2048]{4,3,1,2,0:T(8,128)(2,1)} async-done(((bf16[4,64,1,8,2048]{4,3,1,2,0:T(8,128)(2,1)}), bf16[4,64,1,8,2048]{4,3,1,2,0:T(8,128)(2,1)}, u32[]{:S(2)}, u32[]{:S(2)}) %all-to-all-start.1) | async-done | bytes 8388640 | tf_op jit(solution)/shard_map/all_to_all | solution.py:28
  319.5 7.3 %reduce_sum.63 = bf16[64,8,2048]{2,1,0:T(8,128)(2,1)} reduce(bf16[4,64,1,8,2048]{4,3,1,2,0:T(8,128)(2,1)} %all-to-all-done.1, bf16[]{:T(256)} %constant.96.clone.1), dimensions={0,2}, to_apply=%region_9.10 | reduce | flops 3145728 | bytes 10485762 | tf_op jit(solution)/shard_map/reduce_sum | solution.py:29
  326.8 10.7 %all-to-all-start.2 = ((bf16[64,1,8,2048]{3,2,1,0:T(8,128)(2,1)}), bf16[64,1,8,2048]{3,2,1,0:T(8,128)(2,1)}, u32[]{:S(2)}, u32[]{:S(2)}) async-start(bf16[64,1,8,2048]{3,2,1,0:T(8,128)(2,1)} %bitcast.204), calls=%async_computation.3 | async-start | bytes 4194304 | tf_op jit(solution)/shard_map/all_to_all | solution.py:205
  337.8 2.7 fusion.6
  341.9 2.6 convolution_convert_fusion.1
  345.7 43.0 %all-to-all-done.2 = bf16[64,1,8,2048]{3,2,1,0:T(8,128)(2,1)} async-done(((bf16[64,1,8,2048]{3,2,1,0:T(8,128)(2,1)}), bf16[64,1,8,2048]{3,2,1,0:T(8,128)(2,1)}, u32[]{:S(2)}, u32[]{:S(2)}) %all-to-all-start.2) | async-done | bytes 2097184 | tf_op jit(solution)/shard_map/all_to_all | solution.py:205
  388.7 4.0 bitcast_convert_fusion
  392.7 5.8 %gather_fusion.1 = f32[256,2048]{1,0:T(8,128)} fusion(f32[512,2048]{1,0:T(8,128)} %bitcast_convert_fusion, s32[1024]{0:T(1024)S(1)} %pad_clamp_fusion), kind=kCustom, calls=%fused_computation.1 | custom fusion | bytes 4195328 | tf_op jit(solution)/shard_map/gather | solution.py:210
  398.5 3.5 reshape.468
  402.0 4.7 %multiply_reduce_fusion = f32[128,2048]{1,0:T(8,128)S(1)} fusion(f32[128,2,2048]{2,1,0:T(2,128)} %reshape.468, f32[128,2]{1,0:T(8,128)S(1)} %copy.56), kind=kLoop, calls=%fused_computation.29 | loop fusion | flops 786432 | bytes 3146752 | tf_op jit(solution)/shard_map/reduce_sum | solution.py:211
  (94 shorter events, 19.3 us)
Async XLA Ops:
  7.2 334.8 %copy-start = (bf16[384,2048]{1,0:T(8,128)(2,1)S(1)}, bf16[384,2048]{1,0:T(8,128)(2,1)}, u32[]{:S(2)}) copy-start(bf16[384,2048]{1,0:T(8,128)(2,1)} %param.25) | copy-start | bytes 4718596
  7.2 166.8 %all-gather.2.cloned.1.call-start = ((), (), s32[]{:S(2)}) async-start(), calls=%async_computation.6 | async-start | bytes 10485760 | tf_op jit(solution)/shard_map/all_gather | solution.py:184
  8.3 7.8 %copy-start.8 = (f32[2048]{0:T(1024)S(1)}, f32[2048]{0:T(1024)}, u32[]{:S(2)}) copy-start(f32[2048]{0:T(1024)} %param.20) | copy-start | bytes 24580
  18.3 1.4 copy-start.1
  28.3 145.7 %copy-start.10 = (bf16[1,2048,256]{2,1,0:T(8,128)(2,1)S(1)}, bf16[1,2048,256]{2,1,0:T(8,128)(2,1)}, u32[]{:S(2)}) copy-start(bf16[1,2048,256]{2,1,0:T(8,128)(2,1)} %param.28) | copy-start | bytes 3145732
  203.1 116.4 %all-to-all-start.1 = ((bf16[4,64,1,8,2048]{4,3,1,2,0:T(8,128)(2,1)}), bf16[4,64,1,8,2048]{4,3,1,2,0:T(8,128)(2,1)}, u32[]{:S(2)}, u32[]{:S(2)}) async-start(bf16[4,64,1,8,2048]{4,3,1,2,0:T(8,128)(2,1)} %copy.55), calls=%async_computation.2 | async-start | bytes 16777216 | tf_op jit(solution)/shard_map/all_to_all | solution.py:28
  208.7 2.2 copy-start.11
  208.7 2.2 copy-start.13
  208.8 198.0 %reduce-scatter.5.cloned.1.call-start = ((), (), s32[]{:S(2)}) async-start(), calls=%async_computation.7 | async-start | bytes 2621440 | tf_op jit(solution)/shard_map/reduce_scatter | solution.py:216
  210.9 2.7 copy-start.4
  210.9 2.7 copy-start.12
  213.6 3.4 copy-start.2
  213.6 3.4 copy-start.5
  214.4 3.3 copy-start.6
  214.4 3.3 copy-start.7
  214.8 12.4 %collective-permute-start = (bf16[128,128]{0,1:T(8,128)(2,1)S(1)}, bf16[128,128]{0,1:T(8,128)(2,1)S(1)}, u32[]{:S(2)}, u32[]{:S(2)}) collective-permute-start(bf16[128,128]{0,1:T(8,128)(2,1)S(1)} %pad_maximum_fusion.3), channel_id=1, source_target_pairs={{0,4},{4,8},{8,12},{12,16},{16,20},{20,24},{24,28},{28,32},{32,36}... | collective-permute-start | bytes 98312 | tf_op jit(solution)/shard_map/ppermute | solution.py:17
  227.3 2.3 copy-start.9
  326.8 61.9 %all-to-all-start.2 = ((bf16[64,1,8,2048]{3,2,1,0:T(8,128)(2,1)}), bf16[64,1,8,2048]{3,2,1,0:T(8,128)(2,1)}, u32[]{:S(2)}, u32[]{:S(2)}) async-start(bf16[64,1,8,2048]{3,2,1,0:T(8,128)(2,1)} %bitcast.204), calls=%async_computation.3 | async-start | bytes 4194304 | tf_op jit(solution)/shard_map/all_to_all | solution.py:205
  337.5 71.2 %reduce-scatter.3.cloned.1.call-start = ((), (), s32[]{:S(2)}) async-start(), calls=%async_computation.5 | async-start | bytes 2621440 | tf_op jit(solution)/shard_map/reduce_scatter | solution.py:149
  337.8 2.8 copy-start.3
Sparse Core Ops, SparseCore 0:
  91.9 81.9 all-gather.1
  223.1 51.7 reduce-scatter.4
  344.7 31.4 reduce-scatter.2
where the time goes:
time: 416 us; the launch traced here: 415 us
  waiting for transfers between devices  215 us (52%)
  blocking collectives  63.5 us (15%)
  matrix products  39.2 us (9%)
  local copies, waits for them, and re-layouts  32.7 us (8%)
  other arithmetic  31.7 us (8%)
  starting transfers between devices  18.9 us (5%)
  between operations  14.3 us (3%)
    all_to_all x1, waiting for transfers between devices, sent_and_summed(): lax.all_to_all(pieces, axis, split_axis=0, concat_axis=0, tiled=True)  89.8 us
    all_gather x1, waiting for transfers between devices, local(): lax.all_gather(lax.all_to_all(outgoing, 'ep', split_axis=0, concat_axis=0...  82.2 us
    all_to_all x1, blocking collectives, local(): lax.all_to_all(outgoing, 'ep', split_axis=0, concat_axis=0, tiled=True)  63.5 us
    all_to_all x1, waiting for transfers between devices, local(): lax.all_to_all(summed.astype(jnp.bfloat16), 'ep', split_axis=0, concat_ax...  43 us
    dot_general x1, matrix products, local(): jnp.einsum('iejcf,efd->iejcd', hidden, expert_down, preferred_element_typ...  13.7 us
    all_to_all x1, starting transfers between devices, local(): lax.all_to_all(summed.astype(jnp.bfloat16), 'ep', split_axis=0, concat_ax...  10.7 us
    gather x2, local copies, waits for them, and re-layouts, local(): gathered = returned[own_slot_index().reshape(own_tokens, top_count)]  9.32 us
  transfers between devices with their start and end apart: 6, of which 3 were waited for; matrix products, arithmetic and copies ran while one was open for 13% of the time, Pallas kernels for 0%

commit v1 on v0

--- a/solution.py
+++ b/solution.py
@@ -9,6 +9,14 @@
 SEQS = 1
 norm_eps = 1e-06
 rope_base = 500000.0
+
+
+def tiled_gather(shard, axis, dim):
+    count = lax.axis_size(axis)
+    repeats = [count if d == dim else 1 for d in range(shard.ndim)]
+    return lax.all_to_all(
+        jnp.tile(shard, repeats), axis, split_axis=dim, concat_axis=dim, tiled=True
+    )
 
 
 def from_behind(value, axis, steps):
@@ -181,11 +189,8 @@
         .set(own_owner)
     )
     outgoing = padded_rows[slot_table].reshape(experts_all, 1, capacity, model_width)
-    arrived = lax.all_gather(
-        lax.all_to_all(outgoing, "ep", split_axis=0, concat_axis=0, tiled=True),
-        "tp",
-        axis=1,
-        tiled=True,
+    arrived = tiled_gather(
+        lax.all_to_all(outgoing, "ep", split_axis=0, concat_axis=0, tiled=True), "tp", 1
     )
     sources = arrived.shape[0] // local_experts
     shaped = arrived.reshape(

time: 416 us -> 427 us (1.026)
  blocking collectives: 63.5 us -> 160 us
  waiting for transfers between devices: 215 us -> 130 us
    all_to_all x0 -> x1, blocking collectives: none -> 96.6 us  [tiled_gather(): lax.all_to_all(jnp.tile(shard, repeats), axis, split_axis=dim, concat_axi...]
    all_gather x1 -> x0, waiting for transfers between devices: 82.2 us -> none  [local(): lax.all_gather(lax.all_to_all(outgoing, 'ep', split_axis=0, concat_axis=0...]
  transfers between devices with their start and end apart: 6 -> 5, of which waited for: 3 -> 2; matrix products, arithmetic and copies ran while one was open for 13% -> 13% of each run, Pallas kernels for 0% -> 0%
where the time goes in v1:
time: 427 us
  blocking collectives  160 us (37%)
  waiting for transfers between devices  130 us (30%)
  local copies, waits for them, and re-layouts  36.9 us (9%)
  matrix products  35.3 us (8%)
  other arithmetic  31.8 us (7%)
  starting transfers between devices  17.7 us (4%)
  between operations  14.6 us (3%)
    all_to_all x1, blocking collectives, tiled_gather(): lax.all_to_all(jnp.tile(shard, repeats), axis, split_axis=dim, concat_axi...  96.6 us
    all_to_all x1, waiting for transfers between devices, sent_and_summed(): lax.all_to_all(pieces, axis, split_axis=0, concat_axis=0, tiled=True)  87.3 us
    all_to_all x1, blocking collectives, local(): lax.all_to_all(outgoing, 'ep', split_axis=0, concat_axis=0, tiled=True)  63.3 us
    all_to_all x1, waiting for transfers between devices, local(): lax.all_to_all(summed.astype(jnp.bfloat16), 'ep', split_axis=0, concat_ax...  43 us
    dot_general x1, matrix products, local(): jnp.einsum('iejcf,efd->iejcd', hidden, expert_down, preferred_element_typ...  13.4 us
    all_to_all x1, starting transfers between devices, local(): lax.all_to_all(summed.astype(jnp.bfloat16), 'ep', split_axis=0, concat_ax...  9.46 us
    gather x2, local copies, waits for them, and re-layouts, local(): gathered = returned[own_slot_index().reshape(own_tokens, top_count)]  9.32 us
  transfers between devices with their start and end apart: 5, of which 2 were waited for; matrix products, arithmetic and copies ran while one was open for 13% of the time, Pallas kernels for 0%

profile of v1, /device:TPU:2, one launch (start us, length us, event | category | flops | bytes accessed | tf_op | source)
XLA Modules:
  0.0 426.6 jit_solution(12229963479963203300)
XLA Ops:
  10.6 2.4 reduce-window.6
  21.1 7.1 %gather_fusion = bf16[512,2048]{1,0:T(8,128)(2,1)} fusion(bf16[513,2048]{1,0:T(8,128)(2,1)} %concatenate.64, s32[1024]{0:T(1024)S(1)} %pad_clamp_fusion.1), kind=kCustom, calls=%fused_computation | custom fusion | bytes 4196352 | tf_op jit(solution)/shard_map/gather | solution.py:191
  28.2 63.3 %all_to_all.20 = bf16[64,1,8,2048]{3,2,1,0:T(8,128)(2,1)S(1)} all-to-all(bf16[64,1,8,2048]{3,2,1,0:T(8,128)(2,1)} %bitcast.203), channel_id=1, replica_groups=mesh['ep'=64,'tp'=4] {'ep'}, dimensions={0} | all-to-all | bytes 4194304 | tf_op jit(solution)/shard_map/all_to_all | solution.py:193
  92.6 96.6 %all_to_all.21 = bf16[64,4,8,2048]{3,2,0,1:T(8,128)(2,1)S(1)} all-to-all(bf16[64,4,8,2048]{3,2,0,1:T(8,128)(2,1)S(1)} %tile.10), channel_id=1, replica_groups=mesh['ep'=64,'tp'=4] {'tp'}, dimensions={1} | all-to-all | bytes 16777216 | tf_op jit(solution)/shard_map/all_to_all | solution.py:17
  189.2 3.2 copy-done.3
  192.4 3.6 fusion.2
  196.0 13.4 %convert_bitcast_fusion = bf16[4,64,1,8,2048]{4,3,0,1,2:T(8,128)(2,1)} fusion(bf16[64,4,8,2048]{3,2,0,1:T(8,128)(2,1)} %copy-done.3, f32[64,4,8,256]{3,2,1,0:T(8,128)} %fusion.2, bf16[1,256,2048]{2,1,0:T(8,128)(2,1)S(1)} %copy-done.12, bf16[1,2048,256]{2,1,0:T(8,128)(2,1)} %param.29), kind=kOutput, calls=%fused_computation.3 | convolution fusion | flops 4302307328 | bytes 20971520 | tf_op jit(solution)/shard_map/iejcf,efd->iejcd/dot_general | solution.py:206
  209.5 8.3 %copy.58 = bf16[4,64,1,8,2048]{4,3,1,2,0:T(8,128)(2,1)} copy(bf16[4,64,1,8,2048]{4,3,0,1,2:T(8,128)(2,1)} %convert_bitcast_fusion) | data formatting | bytes 16777216 | tf_op jit(solution)/shard_map/transpose | solution.py:31
  217.7 5.8 %all-to-all-start.2 = ((bf16[4,64,1,8,2048]{4,3,1,2,0:T(8,128)(2,1)}), bf16[4,64,1,8,2048]{4,3,1,2,0:T(8,128)(2,1)}, u32[]{:S(2)}, u32[]{:S(2)}) async-start(bf16[4,64,1,8,2048]{4,3,1,2,0:T(8,128)(2,1)} %copy.58), calls=%async_computation.3 | async-start | bytes 16777216 | tf_op jit(solution)/shard_map/all_to_all | solution.py:36
  223.6 2.2 fusion.4
  225.9 2.4 convolution_convert_fusion.3
  232.5 5.3 %convolution_convert_fusion = bf16[512,2048]{1,0:T(8,128)(2,1)} fusion(bf16[128,2048]{1,0:T(8,128)(2,1)S(1)} %copy-done.7, bf16[512,2048]{1,0:T(8,128)(2,1)} %copy-done.1, bf16[2048,128]{1,0:T(8,128)(2,1)S(1)} %copy-done.8, f32[512,128]{1,0:T(8,128)S(1)} %fusion.94), kind=kOutput, calls=%fused_computation.21 | convolution fusion | flops 538312704 | bytes 5505024 | tf_op jit(solution)/shard_map/dot_general | solution.py:222
  237.8 3.2 convolution_convert_fusion.2
  242.1 2.3 fusion.11
  244.5 87.3 %all-to-all-done.2 = bf16[4,64,1,8,2048]{4,3,1,2,0:T(8,128)(2,1)} async-done(((bf16[4,64,1,8,2048]{4,3,1,2,0:T(8,128)(2,1)}), bf16[4,64,1,8,2048]{4,3,1,2,0:T(8,128)(2,1)}, u32[]{:S(2)}, u32[]{:S(2)}) %all-to-all-start.2) | async-done | bytes 8388640 | tf_op jit(solution)/shard_map/all_to_all | solution.py:36
  331.8 7.3 %reduce_sum.63 = bf16[64,8,2048]{2,1,0:T(8,128)(2,1)} reduce(bf16[4,64,1,8,2048]{4,3,1,2,0:T(8,128)(2,1)} %all-to-all-done.2, bf16[]{:T(256)} %constant.96.clone.1), dimensions={0,2}, to_apply=%region_9.10 | reduce | flops 3145728 | bytes 10485762 | tf_op jit(solution)/shard_map/reduce_sum | solution.py:37
  339.1 9.5 %all-to-all-start.3 = ((bf16[64,1,8,2048]{3,2,1,0:T(8,128)(2,1)}), bf16[64,1,8,2048]{3,2,1,0:T(8,128)(2,1)}, u32[]{:S(2)}, u32[]{:S(2)}) async-start(bf16[64,1,8,2048]{3,2,1,0:T(8,128)(2,1)} %bitcast.205), calls=%async_computation.4 | async-start | bytes 4194304 | tf_op jit(solution)/shard_map/all_to_all | solution.py:210
  348.9 2.7 fusion.10
  353.0 2.6 convolution_convert_fusion.1
  356.7 43.0 %all-to-all-done.3 = bf16[64,1,8,2048]{3,2,1,0:T(8,128)(2,1)} async-done(((bf16[64,1,8,2048]{3,2,1,0:T(8,128)(2,1)}), bf16[64,1,8,2048]{3,2,1,0:T(8,128)(2,1)}, u32[]{:S(2)}, u32[]{:S(2)}) %all-to-all-start.3) | async-done | bytes 2097184 | tf_op jit(solution)/shard_map/all_to_all | solution.py:210
  399.7 4.0 bitcast_convert_fusion
  403.7 5.8 %gather_fusion.1 = f32[256,2048]{1,0:T(8,128)} fusion(f32[512,2048]{1,0:T(8,128)} %bitcast_convert_fusion, s32[1024]{0:T(1024)S(1)} %pad_clamp_fusion), kind=kCustom, calls=%fused_computation.1 | custom fusion | bytes 4195328 | tf_op jit(solution)/shard_map/gather | solution.py:215
  409.5 3.5 reshape.471
  413.1 4.7 %multiply_reduce_fusion = f32[128,2048]{1,0:T(8,128)S(1)} fusion(f32[128,2,2048]{2,1,0:T(2,128)} %reshape.471, f32[128,2]{1,0:T(8,128)S(1)} %copy.59), kind=kLoop, calls=%fused_computation.33 | loop fusion | flops 786432 | bytes 3146752 | tf_op jit(solution)/shard_map/reduce_sum | solution.py:216
  (97 shorter events, 22.5 us)
Async XLA Ops:
  7.2 345.8 %copy-start = (bf16[384,2048]{1,0:T(8,128)(2,1)S(1)}, bf16[384,2048]{1,0:T(8,128)(2,1)}, u32[]{:S(2)}) copy-start(bf16[384,2048]{1,0:T(8,128)(2,1)} %param.25) | copy-start | bytes 4718596
  7.2 8.9 %copy-start.9 = (f32[2048]{0:T(1024)S(1)}, f32[2048]{0:T(1024)}, u32[]{:S(2)}) copy-start(f32[2048]{0:T(1024)} %param.20) | copy-start | bytes 24580
  18.3 1.4 copy-start.1
  92.6 99.8 %copy-start.11 = (bf16[1,2048,256]{2,1,0:T(8,128)(2,1)S(1)}, bf16[1,2048,256]{2,1,0:T(8,128)(2,1)}, u32[]{:S(2)}) copy-start(bf16[1,2048,256]{2,1,0:T(8,128)(2,1)} %param.28) | copy-start | bytes 3145732
  189.2 3.2 copy-start.3
  192.4 3.6 copy-start.12
  217.7 8.1 %copy-start.13 = (bf16[2048,64]{0,1:T(8,128)(2,1)S(1)}, bf16[2048,64]{0,1:T(8,128)(2,1)}, u32[]{:S(2)}) copy-start(bf16[2048,64]{0,1:T(8,128)(2,1)} %param.23) | copy-start | bytes 786436
  217.7 8.1 %copy-start.15 = (f32[2048]{0:T(1024)S(1)}, f32[2048]{0:T(1024)}, u32[]{:S(2)}) copy-start(f32[2048]{0:T(1024)} %param.19) | copy-start | bytes 24580
  217.7 114.1 %all-to-all-start.2 = ((bf16[4,64,1,8,2048]{4,3,1,2,0:T(8,128)(2,1)}), bf16[4,64,1,8,2048]{4,3,1,2,0:T(8,128)(2,1)}, u32[]{:S(2)}, u32[]{:S(2)}) async-start(bf16[4,64,1,8,2048]{4,3,1,2,0:T(8,128)(2,1)} %copy.58), calls=%async_computation.3 | async-start | bytes 16777216 | tf_op jit(solution)/shard_map/all_to_all | solution.py:36
  223.5 4.8 %copy-start.14 = (bf16[2048,64]{0,1:T(8,128)(2,1)S(1)}, bf16[2048,64]{0,1:T(8,128)(2,1)}, u32[]{:S(2)}) copy-start(bf16[2048,64]{0,1:T(8,128)(2,1)} %param.22) | copy-start | bytes 786436
  223.5 194.3 %reduce-scatter.5.cloned.1.call-start = ((), (), s32[]{:S(2)}) async-start(), calls=%async_computation.7 | async-start | bytes 2621440 | tf_op jit(solution)/shard_map/reduce_scatter | solution.py:221
  223.6 4.8 %copy-start.5 = (bf16[512,2048]{1,0:T(8,128)(2,1)S(1)}, bf16[512,2048]{1,0:T(8,128)(2,1)}, u32[]{:S(2)}) copy-start(bf16[512,2048]{1,0:T(8,128)(2,1)} %param.17) | copy-start | bytes 6291460
  228.3 3.5 copy-start.2
  228.3 3.5 copy-start.6
  228.4 4.1 copy-start.7
  228.4 4.1 copy-start.8
  229.6 12.4 %collective-permute-start = (bf16[128,128]{0,1:T(8,128)(2,1)S(1)}, bf16[128,128]{0,1:T(8,128)(2,1)S(1)}, u32[]{:S(2)}, u32[]{:S(2)}) collective-permute-start(bf16[128,128]{0,1:T(8,128)(2,1)S(1)} %pad_maximum_fusion.3), channel_id=1, source_target_pairs={{0,4},{4,8},{8,12},{12,16},{16,20},{20,24},{24,28},{28,32},{32,36}... | collective-permute-start | bytes 98312 | tf_op jit(solution)/shard_map/ppermute | solution.py:25
  241.9 2.5 copy-start.10
  339.1 60.6 %all-to-all-start.3 = ((bf16[64,1,8,2048]{3,2,1,0:T(8,128)(2,1)}), bf16[64,1,8,2048]{3,2,1,0:T(8,128)(2,1)}, u32[]{:S(2)}, u32[]{:S(2)}) async-start(bf16[64,1,8,2048]{3,2,1,0:T(8,128)(2,1)} %bitcast.205), calls=%async_computation.4 | async-start | bytes 4194304 | tf_op jit(solution)/shard_map/all_to_all | solution.py:210
  348.5 71.2 %reduce-scatter.3.cloned.1.call-start = ((), (), s32[]{:S(2)}) async-start(), calls=%async_computation.6 | async-start | bytes 2621440 | tf_op jit(solution)/shard_map/reduce_scatter | solution.py:157
  348.9 2.8 copy-start.4
Sparse Core Ops, SparseCore 0:
  237.9 50.0 reduce-scatter.4
  355.7 31.4 reduce-scatter.2
